TPU v7x, 32 devices: a whole 2x2x4 slice. The times are simulated.
32 devices in a mesh: sp: 8 (over z, x), tp: 4 (over y, core).
Axes of the slice: x: 2, y: 2, z: 4, core: 2. Of those that a mesh axis runs over, the one named last changes fastest.
Arguments:
- x_in: bfloat16 [4096, 1024], P('sp', 'tp'), may hold values from -6 to 6
- gate_b: bfloat16 [4096, 1024], P('sp', 'tp'), may hold values from -6 to 6
- gate_c: bfloat16 [4096, 1024], P('sp', 'tp'), may hold values from -6 to 6
- conv_taps: bfloat16 [3, 1024], P(None, 'tp'), may hold values from -3.5 to 3.5
- out_proj: bfloat16 [1024, 2048], P('tp'), may hold values from -0.1875 to 0.1875
- mix_gain: bfloat16 [2048], replicated, may hold values from 0.099609375 to 1.8984375
- resid: bfloat16 [4096, 2048], P(('sp', 'tp')), may hold values from -6 to 6
- pre_gain: bfloat16 [2048], replicated, may hold values from 0.099609375 to 1.8984375
- expert_gate: bfloat16 [8, 2048, 512], P('sp'), may hold values from -0.125 to 0.125
- expert_up: bfloat16 [8, 2048, 512], P('sp'), may hold values from -0.125 to 0.125
- expert_down: bfloat16 [8, 512, 2048], P('sp'), may hold values from -7.1594562 to 7.1594562
- shared_gate: bfloat16 [2048, 256], replicated, may hold values from -0.125 to 0.125
- shared_up: bfloat16 [2048, 256], replicated, may hold values from -0.125 to 0.125
- shared_down: bfloat16 [256, 2048], replicated, may hold values from -10.125 to 10.125
- post_gain: bfloat16 [2048], replicated, may hold values from 0.099609375 to 1.8984375
- routes: int32 [4096, 4], P(('sp', 'tp')), may hold values from 0 to 7, all different within a row; in each aligned block of 128 rows (0 to 127, 128 to 255, ...) at most 96 rows name the same one
- route_weights: float32 [4096, 4], P(('sp', 'tp')), may hold values from 0.1 to 1
Outputs:
- layer_out: bfloat16 [4096, 2048], P(('sp', 'tp'))
Inputs may be any that keep to these rules, and one draw needn't show every extreme that they name: `routes`: each row names 4 different experts. Within the rows of one device (aligned blocks), no expert is named by more than 96 rows, and in some block one expert is named by exactly 96 rows.
All inputs are finite; a program needn't handle non-finite values.
Results may differ from a plain program's by a relative error of at most 0.007.
Values may be sent and summed in bfloat16 or wider, within the bound.
A program may use at most 128 MiB of HBM per device.

v0:
```python
import jax
import jax.numpy as jnp
from jax import lax
from jax.sharding import PartitionSpec as P

epsilon = 1e-06


def passed_along(shard, axis, by):
    size = lax.axis_size(axis)
    pairs = [(i, i + by) for i in range(size) if 0 <= i + by < size]
    return lax.ppermute(shard, axis, pairs)


def body(
    x_in,
    gate_b,
    gate_c,
    conv_taps,
    out_proj,
    mix_gain,
    resid,
    pre_gain,
    expert_gate,
    expert_up,
    expert_down,
    shared_gate,
    shared_up,
    shared_down,
    post_gain,
    routes,
    route_weights,
):
    row_count = x_in.shape[0]
    channels = x_in.shape[1]
    reach = conv_taps.shape[0] - 1
    edge_rows = jnp.concatenate([x_in[row_count - reach :], gate_c[row_count - reach :]], 1)
    arrived_edge = passed_along(edge_rows, "sp", 1)
    inputs = jnp.concatenate([arrived_edge[:, :channels], x_in], 0).astype(jnp.float32)
    gate_rows = jnp.concatenate([arrived_edge[:, channels:], gate_c], 0).astype(jnp.float32)
    mixed_in = inputs * gate_rows
    taps = conv_taps.astype(jnp.float32)
    convolved = jnp.zeros((row_count, channels), jnp.float32)
    for index in range(reach + 1):
        convolved = convolved + taps[index][None, :] * mixed_in[index : index + row_count]
    conv_out = (gate_b.astype(jnp.float32) * convolved).astype(jnp.bfloat16)
    width_all = out_proj.shape[1]
    full_rows = lax.all_to_all(conv_out, "tp", split_axis=0, concat_axis=1, tiled=True)
    projected = jnp.dot(
        full_rows,
        lax.all_gather(out_proj, "tp", axis=0, tiled=True),
        preferred_element_type=jnp.float32,
    )
    row_scale = lax.rsqrt(jnp.mean(projected * projected, axis=1, keepdims=True) + epsilon)
    resid1 = (
        resid.astype(jnp.float32) + projected * row_scale * mix_gain.astype(jnp.float32)
    ).astype(jnp.bfloat16)
    wide_resid = resid1.astype(jnp.float32)
    normed = (
        wide_resid
        * lax.rsqrt(jnp.mean(wide_resid * wide_resid, axis=1, keepdims=True) + epsilon)
        * pre_gain.astype(jnp.float32)
    ).astype(jnp.bfloat16)
    experts = lax.axis_size("sp")
    local_rows = resid.shape[0]
    top_count = routes.shape[1]
    capacity = 3 * local_rows * top_count // (2 * experts)
    flat_ids = routes.reshape(-1)
    onehot = (flat_ids[:, None] == jnp.arange(experts, dtype=jnp.int32)[None, :]).astype(jnp.int32)
    before = jnp.cumsum(onehot, axis=0) - onehot
    position = jnp.sum(before * onehot, axis=1)
    slot_index = flat_ids * capacity + position
    outgoing = (
        jnp.zeros((experts * capacity, width_all), jnp.bfloat16)
        .at[slot_index]
        .set(jnp.repeat(normed, top_count, axis=0))
    )
    received = lax.all_to_all(
        outgoing.reshape(experts, capacity, width_all),
        "sp",
        split_axis=0,
        concat_axis=0,
        tiled=True,
    )
    arrived = received.reshape(experts * capacity, width_all)
    gate_h = jnp.dot(arrived, expert_gate[0], preferred_element_type=jnp.float32)
    up_h = jnp.dot(arrived, expert_up[0], preferred_element_type=jnp.float32)
    hidden = (jax.nn.silu(gate_h) * up_h).astype(jnp.bfloat16)
    expert_out = jnp.dot(hidden, expert_down[0], preferred_element_type=jnp.float32).astype(
        jnp.bfloat16
    )
    returned = lax.all_to_all(
        expert_out.reshape(experts, capacity, width_all),
        "sp",
        split_axis=0,
        concat_axis=0,
        tiled=True,
    )
    returned = returned.reshape(experts * capacity, width_all)
    picked = returned[slot_index].astype(jnp.float32).reshape(local_rows, top_count, width_all)
    routed = jnp.einsum("tk,tkd->td", route_weights, picked)
    shared_g = jnp.dot(normed, shared_gate, preferred_element_type=jnp.float32)
    shared_u = jnp.dot(normed, shared_up, preferred_element_type=jnp.float32)
    shared_hidden = (jax.nn.silu(shared_g) * shared_u).astype(jnp.bfloat16)
    shared_out = jnp.dot(shared_hidden, shared_down, preferred_element_type=jnp.float32)
    branch = routed + shared_out
    factor = lax.rsqrt(jnp.mean(branch * branch, axis=1, keepdims=True) + epsilon)
    return (wide_resid + branch * factor * post_gain.astype(jnp.float32)[None, :]).astype(
        jnp.bfloat16
    )


def solution(mesh):
    return jax.shard_map(
        body,
        mesh=mesh,
        in_specs=(
            P("sp", "tp"),
            P("sp", "tp"),
            P("sp", "tp"),
            P(None, "tp"),
            P("tp", None),
            P(),
            P(("sp", "tp"), None),
            P(),
            P("sp", None, None),
            P("sp", None, None),
            P("sp", None, None),
            P(),
            P(),
            P(),
            P(),
            P(("sp", "tp"), None),
            P(("sp", "tp"), None),
        ),
        out_specs=P(("sp", "tp"), None),
        check_vma=False,
    )
```

profile of v0, /device:TPU:0, one launch (start us, length us, event | category | flops | bytes accessed | tf_op | source)
XLA Modules:
  0.0 258.1 jit_solution(8605872791199769219)
XLA Ops:
  6.5 0.0 copy-start
  6.5 0.0 copy-start.3
  6.5 0.0 all-gather.2.cloned.1.call-start
  6.5 0.7 all-gather.2.cloned.1.call-update
  7.3 0.7 slice.37
  8.0 0.7 slice.38
  8.7 4.9 %collective-permute-start = (bf16[2,512]{1,0:T(2,128)(2,1)S(1)}, bf16[2,512]{1,0:T(2,128)(2,1)S(1)}, u32[]{:S(2)}, u32[]{:S(2)}) collective-permute-start(bf16[2,512]{1,0:T(2,128)(2,1)S(1)} %pad_maximum_fusion), channel_id=1, source_target_pairs={{0,4},{4,8},{8,12},{12,16},{16,20},{20,24},{24,28},{1,5},{5,9},{9,... | collective-permute-start | bytes 6152 | tf_op jit(solution)/shard_map/ppermute | solution.py:12
  13.5 0.8 copy.23
  14.3 0.1 eq.29
  14.4 0.1 eq.25
  14.6 1.1 reduce-window.6
  15.7 0.2 slice_reduce_fusion
  16.0 0.7 broadcast_multiply_fusion
  16.6 0.8 fusion.31
  17.4 0.1 fusion.27
  17.5 0.7 convert_element_type.62
  18.2 0.7 convert_element_type.67
  18.9 0.1 copy.22
  19.0 0.1 mul.144
  19.1 0.0 collective-permute-done
  19.2 1.2 convert_multiply_fusion.2
  20.4 0.0 copy-done.3
  20.4 0.9 fusion.18
  21.3 3.4 %all-to-all-start = ((bf16[4,128,256]{2,1,0:T(8,128)(2,1)}), bf16[4,128,256]{2,1,0:T(8,128)(2,1)S(1)}, u32[]{:S(2)}, u32[]{:S(2)}) async-start(bf16[4,128,256]{2,1,0:T(8,128)(2,1)} %bitcast.3), calls=%async_computation | async-start | bytes 524288 | tf_op jit(solution)/shard_map/all_to_all | solution.py:48
  24.8 9.2 %all-to-all-done = bf16[4,128,256]{2,1,0:T(8,128)(2,1)S(1)} async-done(((bf16[4,128,256]{2,1,0:T(8,128)(2,1)}), bf16[4,128,256]{2,1,0:T(8,128)(2,1)S(1)}, u32[]{:S(2)}, u32[]{:S(2)}) %all-to-all-start) | async-done | bytes 262176 | tf_op jit(solution)/shard_map/all_to_all | solution.py:48
  33.9 0.2 copy.21
  34.1 14.8 %all-gather.2.cloned.1.call-done = bf16[1024,2048]{1,0:T(8,128)(2,1)} async-done(((bf16[256,2048]{1,0:T(8,128)(2,1)}), bf16[1024,2048]{1,0:T(8,128)(2,1)}) %all-gather.2.cloned.1.call-update) | async-done | bytes 4194320 | tf_op jit(solution)/shard_map/all_gather | solution.py:51
  48.9 0.0 copy-start.2
  48.9 3.1 %multiply_reduce_fusion.1 = (f32[128]{0:T(128)S(1)}, f32[128,2048]{1,0:T(8,128)S(1)}) fusion(bf16[128,1024]{0,1:T(8,128)(2,1)S(1)} %bitcast.51, bf16[1024,2048]{1,0:T(8,128)(2,1)} %all-gather.2.cloned.1.call-done), kind=kOutput, calls=%fused_computation.23 | convolution fusion | flops 537395072 | bytes 5505536 | tf_op jit(solution)/shard_map/dot_general | solution.py:49
  52.0 0.0 copy-done.2
  52.0 0.4 fusion.10
  52.4 0.2 fusion.12
  52.6 2.4 broadcast_in_dim.5
  55.0 4.0 %reshape.113 = bf16[512,2048]{1,0:T(8,128)(2,1)} reshape(bf16[128,4,2048]{2,1,0:T(4,128)(2,1)} %broadcast_in_dim.5) | data formatting | bytes 4194304 | tf_op jit(solution)/shard_map/reshape | solution.py:76
  59.0 6.7 %scatter_custom_fusion = bf16[768,2048]{1,0:T(8,128)(2,1)} fusion(s32[512]{0:T(512)S(1)} %bitcast.53, bf16[512,2048]{1,0:T(8,128)(2,1)} %reshape.113, bf16[]{:T(256)} %constant.22.clone.1), kind=kCustom, calls=%fused_computation.10 | custom fusion | bytes 3146240 | tf_op jit(solution)/shard_map/scatter | solution.py:76
  65.7 0.0 copy-start.6
  65.7 76.7 %all_to_all.29 = bf16[8,96,2048]{2,1,0:T(8,128)(2,1)S(1)} all-to-all(bf16[8,96,2048]{2,1,0:T(8,128)(2,1)} %bitcast.47), channel_id=1, replica_groups=mesh['sp'=8,'tp'=4] {'sp'}, dimensions={0} | all-to-all | bytes 6291456 | tf_op jit(solution)/shard_map/all_to_all | solution.py:78
  142.4 0.0 copy-start.1
  142.4 1.7 copy-done.1
  144.1 0.0 copy-done.6
  144.1 2.9 %fusion.3 = f32[768,512]{1,0:T(8,128)} fusion(bf16[768,2048]{1,0:T(8,128)(2,1)S(1)} %bitcast.49, bf16[1,2048,512]{2,1,0:T(8,128)(2,1)S(1)} %copy-done.6), kind=kOutput, calls=%fused_computation.7 | convolution fusion | flops 1610612736 | bytes 6815744 | tf_op jit(solution)/shard_map/dot_general | solution.py:86
  147.0 0.0 copy-done
  147.0 8.1 %convolution_convert_fusion = bf16[768,2048]{1,0:T(8,128)(2,1)} fusion(bf16[1,512,2048]{2,1,0:T(8,128)(2,1)S(1)} %copy-done, f32[768,512]{1,0:T(8,128)} %fusion.3, bf16[768,2048]{1,0:T(8,128)(2,1)} %bitcast.50, bf16[1,2048,512]{2,1,0:T(8,128)(2,1)} %param.26), kind=kOutput, calls=%fused_computation.2 | convolution fusion | flops 3225157632 | bytes 12058624 | tf_op jit(solution)/shard_map/dot_general | solution.py:89
  155.2 0.0 copy-start.5
  155.2 0.0 copy-start.4
  155.2 4.8 %all-to-all-start.2 = ((bf16[8,96,2048]{2,1,0:T(8,128)(2,1)}), bf16[8,96,2048]{2,1,0:T(8,128)(2,1)}, u32[]{:S(2)}, u32[]{:S(2)}) async-start(bf16[8,96,2048]{2,1,0:T(8,128)(2,1)} %bitcast.48), calls=%async_computation.2 | async-start | bytes 6291456 | tf_op jit(solution)/shard_map/all_to_all | solution.py:92
  160.0 0.0 copy-done.5
  160.0 0.2 copy.25
  160.1 0.0 copy-done.4
  160.2 1.5 fusion.34
  161.7 68.1 %all-to-all-done.2 = bf16[8,96,2048]{2,1,0:T(8,128)(2,1)} async-done(((bf16[8,96,2048]{2,1,0:T(8,128)(2,1)}), bf16[8,96,2048]{2,1,0:T(8,128)(2,1)}, u32[]{:S(2)}, u32[]{:S(2)}) %all-to-all-start.2) | async-done | bytes 3145760 | tf_op jit(solution)/shard_map/all_to_all | solution.py:92
  229.8 7.6 %gather_fusion = bf16[512,2048]{1,0:T(8,128)(2,1)} fusion(bf16[768,2048]{1,0:T(8,128)(2,1)} %bitcast.16, s32[1024]{0:T(1024)S(1)} %pad_clamp_fusion), kind=kCustom, calls=%fused_computation | custom fusion | bytes 4196352 | tf_op jit(solution)/shard_map/gather | solution.py:100
  237.3 4.1 %reshape.100 = bf16[128,4,2048]{2,1,0:T(4,128)(2,1)} reshape(bf16[512,2048]{1,0:T(8,128)(2,1)} %gather_fusion) | data formatting | bytes 4194304 | tf_op jit(solution)/shard_map/reshape | solution.py:100
  241.5 3.8 %fusion.33 = f32[128,1,2048]{2,1,0:T(1,128)} fusion(bf16[128,4,2048]{2,1,0:T(4,128)(2,1)} %reshape.100, bf16[128,4,1]{1,2,0:T(2,128)(2,1)S(1)} %copy.25), kind=kOutput, calls=%fused_computation.56 | convolution fusion | flops 2097152 | bytes 3146752 | tf_op jit(solution)/shard_map/tk,tkd->td/dot_general | solution.py:101
  245.3 3.8 %multiply_reduce_fusion = (f32[128]{0:T(128)S(1)}, f32[128,2048]{1,0:T(8,128)}) fusion(bf16[256,2048]{1,0:T(8,128)(2,1)} %param.30, bf16[128,2048]{1,0:T(8,128)(2,1)S(1)} %fusion.12, bf16[2048,256]{1,0:T(8,128)(2,1)} %param.29, f32[128,256]{1,0:T(8,128)S(1)} %fusion.34, f32[128,1,2048]{2,1,0:T(1,128)} %fusion.33), kind=kOutput, calls=%fused_computation.21 | convolution fusion | flops 269418368 | bytes 4850176 | tf_op jit(solution)/shard_map/dot_general | solution.py:105
  249.0 2.2 fusion.13
  (11 shorter events, 0.1 us)
Async XLA Ops:
  6.5 140.5 %copy-start = (bf16[1,512,2048]{2,1,0:T(8,128)(2,1)S(1)}, bf16[1,512,2048]{2,1,0:T(8,128)(2,1)}, u32[]{:S(2)}) copy-start(bf16[1,512,2048]{2,1,0:T(8,128)(2,1)} %param.27) | copy-start | bytes 6291460
  6.5 13.9 %copy-start.3 = (bf16[512,256]{1,0:T(8,128)(2,1)S(1)}, bf16[512,256]{1,0:T(8,128)(2,1)}, u32[]{:S(2)}) copy-start(bf16[512,256]{1,0:T(8,128)(2,1)} %param.18) | copy-start | bytes 786436
  6.5 42.4 %all-gather.2.cloned.1.call-start = ((), (), s32[]{:S(2)}) async-start(), calls=%async_computation.3 | async-start | bytes 5242880 | tf_op jit(solution)/shard_map/all_gather | solution.py:51
  8.7 10.5 %collective-permute-start = (bf16[2,512]{1,0:T(2,128)(2,1)S(1)}, bf16[2,512]{1,0:T(2,128)(2,1)S(1)}, u32[]{:S(2)}, u32[]{:S(2)}) collective-permute-start(bf16[2,512]{1,0:T(2,128)(2,1)S(1)} %pad_maximum_fusion), channel_id=1, source_target_pairs={{0,4},{4,8},{8,12},{12,16},{16,20},{20,24},{24,28},{1,5},{5,9},{9,... | collective-permute-start | bytes 6152 | tf_op jit(solution)/shard_map/ppermute | solution.py:12
  21.3 12.6 %all-to-all-start = ((bf16[4,128,256]{2,1,0:T(8,128)(2,1)}), bf16[4,128,256]{2,1,0:T(8,128)(2,1)S(1)}, u32[]{:S(2)}, u32[]{:S(2)}) async-start(bf16[4,128,256]{2,1,0:T(8,128)(2,1)} %bitcast.3), calls=%async_computation | async-start | bytes 524288 | tf_op jit(solution)/shard_map/all_to_all | solution.py:48
  48.9 3.1 %copy-start.2 = (bf16[128,2048]{1,0:T(8,128)(2,1)S(1)}, bf16[128,2048]{1,0:T(8,128)(2,1)}, u32[]{:S(2)}) copy-start(bf16[128,2048]{1,0:T(8,128)(2,1)} %param.23) | copy-start | bytes 1572868
  65.7 78.4 %copy-start.6 = (bf16[1,2048,512]{2,1,0:T(8,128)(2,1)S(1)}, bf16[1,2048,512]{2,1,0:T(8,128)(2,1)}, u32[]{:S(2)}) copy-start(bf16[1,2048,512]{2,1,0:T(8,128)(2,1)} %param.25) | copy-start | bytes 6291460
  142.4 1.7 copy-start.1
  155.2 4.8 %copy-start.5 = (f32[128,4]{0,1:T(4,128)S(1)}, f32[128,4]{0,1:T(4,128)}, u32[]{:S(2)}) copy-start(f32[128,4]{0,1:T(4,128)} %param.33) | copy-start | bytes 6148
  155.2 4.9 %copy-start.4 = (bf16[2048]{0:T(1024)(128)(2,1)S(1)}, bf16[2048]{0:T(1024)(128)(2,1)}, u32[]{:S(2)}) copy-start(bf16[2048]{0:T(1024)(128)(2,1)} %param.31) | copy-start | bytes 12292
  155.2 74.6 %all-to-all-start.2 = ((bf16[8,96,2048]{2,1,0:T(8,128)(2,1)}), bf16[8,96,2048]{2,1,0:T(8,128)(2,1)}, u32[]{:S(2)}, u32[]{:S(2)}) async-start(bf16[8,96,2048]{2,1,0:T(8,128)(2,1)} %bitcast.48), calls=%async_computation.2 | async-start | bytes 6291456 | tf_op jit(solution)/shard_map/all_to_all | solution.py:92
Sparse Core Ops, SparseCore 0:
  8.9 39.9 all-gather.1
where the time goes:
time: 259 us; the launch traced here: 258 us
  waiting for transfers between devices  92.8 us (36%)
  blocking collectives  76.7 us (30%)
  local copies, waits for them, and re-layouts  30.5 us (12%)
  matrix products  23.2 us (9%)
  between operations  13.6 us (5%)
  starting transfers between devices  13 us (5%)
  other arithmetic  8.37 us (3%)
    all_to_all x1, blocking collectives, body(): lax.all_to_all(outgoing.reshape(experts, capacity, width_all), 'sp', spli...  76.7 us
    all_to_all x1, waiting for transfers between devices, body(): lax.all_to_all(expert_out.reshape(experts, capacity, width_all), 'sp', sp...  68.1 us
    all_gather x1, waiting for transfers between devices, body(): lax.all_gather(out_proj, 'tp', axis=0, tiled=True)  14.8 us
    all_to_all x1, waiting for transfers between devices, body(): lax.all_to_all(conv_out, 'tp', split_axis=0, concat_axis=1, tiled=True)  9.18 us
    dot_general x1, matrix products, body(): jnp.dot(hidden, expert_down[0], preferred_element_type=jnp.float32)  8.14 us
    gather x1, local copies, waits for them, and re-layouts, body(): returned[slot_index].astype(jnp.float32)  7.58 us
    scatter x1, local copies, waits for them, and re-layouts, body(): outgoing = jnp.zeros((experts * capacity, width_all), jnp.bfloat16).at[sl...  6.71 us
  transfers between devices with their start and end apart: 4, of which 3 were waited for; matrix products, arithmetic and copies ran while one was open for 4% of the time, Pallas kernels for 0%

commit v1 on v0

--- a/solution.py
+++ b/solution.py
@@ -1,9 +1,419 @@
+import functools
+
 import jax
 import jax.numpy as jnp
 from jax import lax
-from jax.sharding import PartitionSpec as P
-
+from jax.experimental import pallas as pl
+from jax.experimental.pallas import tpu as pltpu
+
+P = jax.sharding.PartitionSpec
+MESH = pl.DeviceIdType.MESH
 epsilon = 1e-06
+PIECES = 4
+HALVES = 2
+
+
+def moe_kernel(
+    line,
+    normed_ref,
+    resid_ref,
+    routes_ref,
+    weights_ref,
+    post_ref,
+    eg_ref,
+    eu_ref,
+    ed_ref,
+    sg_ref,
+    su_ref,
+    sd_ref,
+    out_ref,
+    w_gate,
+    w_up,
+    w_down,
+    s_gate,
+    s_up,
+    s_down,
+    blocks,
+    sums,
+    shared,
+    from_low,
+    from_high,
+    outgoing,
+    shares,
+    hidden,
+    load_sem,
+    wx_send,
+    wx_recv,
+    wn_send,
+    wn_recv,
+    wf_send,
+    wf_recv,
+    wr_send,
+    wr_recv,
+    t_send,
+    t_recv,
+    gu_send,
+    gu_recv,
+    gd_send,
+    gd_recv,
+    ru_send,
+    ru_recv,
+    rd_send,
+    rd_recv,
+):
+    sp = lax.axis_index("sp")
+    tp = lax.axis_index("tp")
+    sp_size = lax.axis_size("sp")
+    tp_size = lax.axis_size("tp")
+    z = sp // 2
+    x = sp % 2
+    last = line - 1
+    mate = z * 2 + 1 - x
+    near = (tp // 2) * 2 + 1 - tp % 2
+    far = (tp + 2) % tp_size
+    near_far = (near + 2) % tp_size
+    rows, width = normed_ref.shape
+    step_rows = rows // PIECES
+    hid = w_gate.shape[2]
+    shared_hid = s_gate.shape[1]
+
+    barrier = pltpu.get_barrier_semaphore()
+    for k in range(1, sp_size):
+        pl.semaphore_signal(barrier, inc=1, device_id=((sp + k) % sp_size, tp), device_id_type=MESH)
+    for k in range(1, tp_size):
+        pl.semaphore_signal(barrier, inc=1, device_id=(sp, (tp + k) % tp_size), device_id_type=MESH)
+
+    loads = [
+        pltpu.make_async_copy(src, dst, load_sem.at[n])
+        for n, (src, dst) in enumerate(
+            (
+                (eg_ref.at[0], w_gate.at[0]),
+                (eu_ref.at[0], w_up.at[0]),
+                (ed_ref.at[0], w_down.at[0]),
+                (sg_ref, s_gate),
+                (su_ref, s_up),
+                (sd_ref, s_down),
+            )
+        )
+    ]
+    for load in loads:
+        load.start()
+    pl.semaphore_wait(barrier, sp_size - 1 + tp_size - 1)
+
+    pieces = []
+    for ref, held in ((eg_ref, w_gate), (eu_ref, w_up), (ed_ref, w_down)):
+        size = ref.shape[1] // tp_size // HALVES
+        for h in range(HALVES):
+            pieces.append((ref, held, size, h))
+
+    def span(owner, n):
+        _, _, size, h = pieces[n]
+        return pl.ds(pl.multiple_of((owner * HALVES + h) * size, size), size)
+
+    def hop(n, owner, target, send, recv, first=False):
+        ref, held, _, _ = pieces[n]
+        where = span(owner, n)
+        return pltpu.make_async_remote_copy(
+            src_ref=ref.at[0, where] if first else held.at[1, where],
+            dst_ref=held.at[1, where],
+            send_sem=send.at[n],
+            recv_sem=recv.at[n],
+            device_id=target,
+            device_id_type=MESH,
+        )
+
+    def x_hop(n):
+        return hop(n, tp, (mate, tp), wx_send, wx_recv, True)
+
+    def near_hop(n, owner):
+        return hop(n, owner, (sp, near), wn_send, wn_recv)
+
+    def far_hop(n, owner):
+        return hop(n, owner, (sp, far), wf_send, wf_recv)
+
+    def relay_hop(n, owner):
+        return hop(n, owner, (sp, near), wr_send, wr_recv)
+
+    count = len(pieces)
+
+    def line_copy(source, landing, b, c, up, send, recv):
+        part = pl.ds(pl.multiple_of(c * step_rows, step_rows), step_rows)
+        return pltpu.make_async_remote_copy(
+            src_ref=source.at[b, part],
+            dst_ref=landing.at[b, part],
+            send_sem=send.at[b, c],
+            recv_sem=recv.at[b, c],
+            device_id=((z + (1 if up else -1)) * 2 + x, tp),
+            device_id_type=MESH,
+        )
+
+    def go_up(b, c):
+        return line_copy(blocks, blocks, b, c, True, gu_send, gu_recv)
+
+    def go_down(b, c):
+        return line_copy(blocks, blocks, b, c, False, gd_send, gd_recv)
+
+    def back_up(b, c):
+        return line_copy(outgoing, from_low, b, c, True, ru_send, ru_recv)
+
+    def back_down(b, c):
+        return line_copy(outgoing, from_high, b, c, False, rd_send, rd_recv)
+
+    def share_copy(k, source):
+        return pltpu.make_async_remote_copy(
+            src_ref=shares.at[source],
+            dst_ref=shares.at[source],
+            send_sem=t_send.at[k],
+            recv_sem=t_recv.at[source],
+            device_id=(((z + k) % line) * 2 + x, tp),
+            device_id_type=MESH,
+        )
+
+    lanes = lax.broadcasted_iota(jnp.int32, (rows, shares.shape[2]), 1)
+    table = jnp.zeros((rows, shares.shape[2]), jnp.float32)
+    for k in range(routes_ref.shape[1]):
+        table += jnp.where(lanes == routes_ref[:, k : k + 1], weights_ref[:, k : k + 1], 0.0)
+    shares[z] = table
+    blocks[z] = normed_ref[...]
+    sums[...] = jnp.zeros_like(sums)
+    for c in range(PIECES):
+
+        @pl.when(z < last)
+        def _():
+            go_up(z, c).start()
+
+        @pl.when(z > 0)
+        def _():
+            go_down(z, c).start()
+
+    for n in range(count):
+        x_hop(n).start()
+    for k in range(1, line):
+        share_copy(k, z).start()
+
+    def apply(b, i):
+        expert = z * 2 + x + i * (1 - 2 * x)
+
+        @pl.loop(0, hid // 256)
+        def _(j):
+            cols = pl.ds(pl.multiple_of(j * 256, 256), 256)
+            gate = jnp.dot(blocks[b], w_gate[i, :, cols], preferred_element_type=jnp.float32)
+            up = jnp.dot(blocks[b], w_up[i, :, cols], preferred_element_type=jnp.float32)
+            hidden[:, cols] = (jax.nn.silu(gate) * up).astype(jnp.bfloat16)
+
+        share = jnp.sum(jnp.where(lanes == expert, shares[b], 0.0), axis=1, keepdims=True)
+
+        @pl.loop(0, width // 512)
+        def _(j):
+            cols = pl.ds(pl.multiple_of(j * 512, 512), 512)
+            made = jnp.dot(hidden[...], w_down[i, :, cols], preferred_element_type=jnp.float32)
+            made = made.astype(jnp.bfloat16).astype(jnp.float32)
+            sums[b, :, cols] += jnp.where(share > 0.0, share * made, 0.0)
+
+    def receive(t):
+        @pl.loop(0, PIECES)
+        def _(c):
+            @pl.when(z - t >= 0)
+            def _():
+                go_up(z - t, c).wait_recv()
+
+                @pl.when(z < last)
+                def _():
+                    go_up(z - t, c).start()
+
+            @pl.when(z + t <= last)
+            def _():
+                go_down(z + t, c).wait_recv()
+
+                @pl.when(z > 0)
+                def _():
+                    go_down(z + t, c).start()
+
+    def apply_pair(t, i):
+        @pl.loop(0, 2)
+        def _(side):
+            b = z - t + side * 2 * t
+
+            @pl.when((b >= 0) & (b <= last))
+            def _():
+                apply(b, i)
+
+    def give_back(t):
+        b_up = t - z
+        b_down = 2 * last - z - t
+
+        @pl.loop(0, PIECES)
+        def _(c):
+            part = pl.ds(pl.multiple_of(c * step_rows, step_rows), step_rows)
+
+            @pl.when((b_up > z) & (b_up <= last))
+            def _():
+                @pl.when(z > 0)
+                def _():
+                    back_up(b_up, c).wait_recv()
+                    sums[b_up, part] += from_low[b_up, part].astype(jnp.float32)
+
+                outgoing[b_up, part] = sums[b_up, part].astype(jnp.bfloat16)
+                back_up(b_up, c).start()
+
+            @pl.when((b_down < z) & (b_down >= 0))
+            def _():
+                @pl.when(z < last)
+                def _():
+                    back_down(b_down, c).wait_recv()
+                    sums[b_down, part] += from_high[b_down, part].astype(jnp.float32)
+
+                outgoing[b_down, part] = sums[b_down, part].astype(jnp.bfloat16)
+                back_down(b_down, c).start()
+
+    for load in loads[:3]:
+        load.wait()
+    apply(z, 0)
+    for load in loads[3:]:
+        load.wait()
+    s_g = jnp.dot(blocks[z], s_gate[...], preferred_element_type=jnp.float32)
+    s_u = jnp.dot(blocks[z], s_up[...], preferred_element_type=jnp.float32)
+    s_h = (jax.nn.silu(s_g) * s_u).astype(jnp.bfloat16)
+    hidden[:, :shared_hid] = s_h
+
+    @pl.loop(0, width // 512)
+    def _(j):
+        cols = pl.ds(pl.multiple_of(j * 512, 512), 512)
+        shared[:, cols] = jnp.dot(
+            hidden[:, :shared_hid], s_down[:, cols], preferred_element_type=jnp.float32
+        )
+
+    for n in range(count):
+        x_hop(n).wait_recv()
+        far_hop(n, tp).start()
+        near_hop(n, tp).start()
+    receive(1)
+    for k in range(1, line):
+        share_copy(k, (z + k) % line).wait_recv()
+    apply_pair(1, 0)
+    for n in range(count):
+        far_hop(n, far).wait_recv()
+        relay_hop(n, far).start()
+    receive(2)
+    for n in range(count):
+        near_hop(n, near).wait_recv()
+        relay_hop(n, near_far).wait_recv()
+    apply_pair(1, 1)
+    give_back(1)
+
+    @pl.loop(2, line)
+    def _(t):
+        @pl.when(t > 2)
+        def _():
+            receive(t)
+
+        apply_pair(t, 0)
+        apply_pair(t, 1)
+        give_back(t)
+
+    apply(z, 1)
+
+    @pl.loop(line, 2 * line - 2)
+    def _(t):
+        give_back(t)
+
+    @pl.loop(0, PIECES)
+    def _(c):
+        part = pl.ds(pl.multiple_of(c * step_rows, step_rows), step_rows)
+
+        @pl.when(z > 0)
+        def _():
+            back_up(z, c).wait_recv()
+            sums[z, part] += from_low[z, part].astype(jnp.float32)
+
+        @pl.when(z < last)
+        def _():
+            back_down(z, c).wait_recv()
+            sums[z, part] += from_high[z, part].astype(jnp.float32)
+
+        branch = sums[z, part] + shared[part]
+        factor = lax.rsqrt(jnp.mean(branch * branch, axis=1, keepdims=True) + epsilon)
+        out_ref[part] = (
+            resid_ref[part].astype(jnp.float32)
+            + branch * factor * post_ref[...].astype(jnp.float32)
+        ).astype(jnp.bfloat16)
+
+    for n in range(count):
+        x_hop(n).wait_send()
+        near_hop(n, tp).wait_send()
+        far_hop(n, tp).wait_send()
+        relay_hop(n, far).wait_send()
+    for k in range(1, line):
+        share_copy(k, z).wait_send()
+
+    @pl.loop(0, PIECES)
+    def _(c):
+        @pl.loop(0, line)
+        def _(b):
+            @pl.when((b <= z) & (z < last))
+            def _():
+                go_up(b, c).wait_send()
+
+            @pl.when((b >= z) & (z > 0))
+            def _():
+                go_down(b, c).wait_send()
+
+            @pl.when(b > z)
+            def _():
+                back_up(b, c).wait_send()
+
+            @pl.when(b < z)
+            def _():
+                back_down(b, c).wait_send()
+
+
+def routed_and_shared(
+    normed, resid1, routes, route_weights, post_gain, expert_gate, expert_up, expert_down,
+    shared_gate, shared_up, shared_down,
+):
+    experts = lax.axis_size("sp")
+    line = experts // 2
+    rows, width = normed.shape
+    hid = expert_gate.shape[2]
+    shared_hid = shared_gate.shape[1]
+    dma = pltpu.SemaphoreType.DMA
+    count = 3 * HALVES
+    bf, f32 = jnp.bfloat16, jnp.float32
+    vmem = pl.BlockSpec(memory_space=pltpu.VMEM)
+    anywhere = pl.BlockSpec(memory_space=pltpu.HBM)
+    lanes = 128 * (-(-experts // 128))
+    return pl.pallas_call(
+        functools.partial(moe_kernel, line),
+        out_shape=jax.ShapeDtypeStruct((rows, width), bf),
+        in_specs=[vmem] * 5 + [anywhere] * 6,
+        out_specs=vmem,
+        scratch_shapes=[
+            pltpu.VMEM((2, width, hid), bf),
+            pltpu.VMEM((2, width, hid), bf),
+            pltpu.VMEM((2, hid, width), bf),
+            pltpu.VMEM((width, shared_hid), bf),
+            pltpu.VMEM((width, shared_hid), bf),
+            pltpu.VMEM((shared_hid, width), bf),
+            pltpu.VMEM((line, rows, width), bf),
+            pltpu.VMEM((line, rows, width), f32),
+            pltpu.VMEM((rows, width), f32),
+            pltpu.VMEM((line, rows, width), bf),
+            pltpu.VMEM((line, rows, width), bf),
+            pltpu.VMEM((line, rows, width), bf),
+            pltpu.VMEM((line, rows, lanes), f32),
+            pltpu.VMEM((rows, max(hid, shared_hid)), bf),
+            dma((6,)),
+        ]
+        + [dma((count,))] * 8
+        + [dma((line,))] * 2
+        + [dma((line, PIECES))] * 8,
+        compiler_params=pltpu.CompilerParams(
+            collective_id=0, has_side_effects=True, vmem_limit_bytes=60 * 1024 * 1024
+        ),
+    )(
+        normed, resid1, routes, route_weights, post_gain.reshape(1, width),
+        expert_gate, expert_up, expert_down, shared_gate, shared_up, shared_down,
+    )
 
 
 def passed_along(shard, axis, by):
@@ -65,6 +475,11 @@
     local_rows = resid.shape[0]
     top_count = routes.shape[1]
     capacity = 3 * local_rows * top_count // (2 * experts)
+    if 2 * capacity > local_rows and experts % 2 == 0 and lax.axis_size("tp") == 2 * 2:
+        return routed_and_shared(
+            normed, resid1, routes, route_weights, post_gain, expert_gate, expert_up, expert_down,
+            shared_gate, shared_up, shared_down,
+        )
     flat_ids = routes.reshape(-1)
     onehot = (flat_ids[:, None] == jnp.arange(experts, dtype=jnp.int32)[None, :]).astype(jnp.int32)
     before = jnp.cumsum(onehot, axis=0) - onehot

time: 259 us -> 165 us (0.64)
  Pallas kernels: 0 us -> 103 us
  blocking collectives: 76.7 us -> 0 us
  waiting for transfers between devices: 92.8 us -> 26.5 us
  local copies, waits for them, and re-layouts: 30.5 us -> 6.32 us
  matrix products: 23.2 us -> 3 us
  starting transfers between devices: 13 us -> 8.34 us
  other arithmetic: 8.37 us -> 4.46 us
    pallas_call x0 -> x1, Pallas kernels: none -> 103 us  [routed_and_shared(): pl.pallas_call(functools.partial(moe_kernel, line), out_shape=jax.ShapeDt...]
    all_to_all x1 -> x0, blocking collectives: 76.7 us -> none  [body(): lax.all_to_all(outgoing.reshape(experts, capacity, width_all), 'sp', spli...]
    all_to_all x1 -> x0, waiting for transfers between devices: 68.1 us -> none  [body(): lax.all_to_all(expert_out.reshape(experts, capacity, width_all), 'sp', sp...]
    dot_general x5 -> x0, matrix products: 20.2 us -> none  [the longest x1 8.14 us: body(): jnp.dot(hidden, expert_down[0], preferred_element_type=jnp.float32)]
    gather x1 -> x0, local copies, waits for them, and re-layouts: 7.58 us -> none  [body(): returned[slot_index].astype(jnp.float32)]
    reshape x2 -> x1, local copies, waits for them, and re-layouts: 8.08 us -> 0.59 us  [routed_and_shared(): post_gain.reshape(1, width)]
    scatter x1 -> x0, local copies, waits for them, and re-layouts: 6.71 us -> none  [body(): outgoing = jnp.zeros((experts * capacity, width_all), jnp.bfloat16).at[sl...]
    all_to_all x1 -> x0, starting transfers between devices: 4.75 us -> none  [body(): lax.all_to_all(expert_out.reshape(experts, capacity, width_all), 'sp', sp...]
  transfers between devices with their start and end apart: 4 -> 3, of which waited for: 3 -> 3; matrix products, arithmetic and copies ran while one was open for 4% -> 5% of each run, Pallas kernels for 0% -> 0%
where the time goes in v1:
time: 165 us
  Pallas kernels  103 us (62%)
  waiting for transfers between devices  26.5 us (16%)
  between operations  13.5 us (8%)
  starting transfers between devices  8.34 us (5%)
  local copies, waits for them, and re-layouts  6.32 us (4%)
  other arithmetic  4.46 us (3%)
  matrix products  3 us (2%)
    pallas_call x1, Pallas kernels, routed_and_shared(): pl.pallas_call(functools.partial(moe_kernel, line), out_shape=jax.ShapeDt...  103 us
    all_gather x1, waiting for transfers between devices, body(): lax.all_gather(out_proj, 'tp', axis=0, tiled=True)  18.2 us
    all_to_all x1, waiting for transfers between devices, body(): lax.all_to_all(conv_out, 'tp', split_axis=0, concat_axis=1, tiled=True)  7.09 us
    ppermute x1, starting transfers between devices, passed_along(): return lax.ppermute(shard, axis, pairs)  4.87 us
    all_to_all x1, starting transfers between devices, body(): lax.all_to_all(conv_out, 'tp', split_axis=0, concat_axis=1, tiled=True)  3.44 us
    unnamed x17, local copies, waits for them, and re-layouts  3.36 us
  transfers between devices with their start and end apart: 3, of which 3 were waited for; matrix products, arithmetic and copies ran while one was open for 5% of the time, Pallas kernels for 0%

profile of v1, /device:TPU:0, one launch (start us, length us, event | category | flops | bytes accessed | tf_op | source)
XLA Modules:
  0.0 164.8 jit_solution(14279266020629347650)
XLA Ops:
  6.5 0.0 copy-start.2
  6.5 0.0 copy-start.3
  6.5 0.0 copy-start.5
  6.5 0.0 copy-start.6
  6.5 0.0 copy-start.4
  6.5 0.0 all-gather.2.cloned.1.call-start
  6.6 0.7 all-gather.2.cloned.1.call-update
  7.3 0.7 slice.31
  8.0 0.7 slice.32
  8.7 4.9 %collective-permute-start = (bf16[2,512]{1,0:T(2,128)(2,1)S(1)}, bf16[2,512]{1,0:T(2,128)(2,1)S(1)}, u32[]{:S(2)}, u32[]{:S(2)}) collective-permute-start(bf16[2,512]{1,0:T(2,128)(2,1)S(1)} %pad_maximum_fusion), channel_id=1, source_target_pairs={{0,4},{4,8},{8,12},{12,16},{16,20},{20,24},{24,28},{1,5},{5,9},{9,... | collective-permute-start | bytes 6152 | tf_op jit(solution)/shard_map/ppermute | solution.py:422
  13.6 0.8 fusion.7
  14.4 0.5 collective-permute-done
  14.9 1.2 convert_multiply_fusion.2
  16.0 0.0 copy-start.1
  16.0 1.9 %fusion.5 = bf16[512,256]{1,0:T(8,128)(2,1)} fusion(f32[514,256]{1,0:T(8,128)S(1)} %convert_multiply_fusion.2, bf16[512,256]{1,0:T(8,128)(2,1)} %param.18, f32[256]{0:T(256)S(1)} %bitcast.12, f32[256]{0:T(256)S(1)} %bitcast.11, f32[256]{0:T(256)S(1)} %bitcast.10), kind=kLoop, calls=%fused_computation.11 | loop fusion | flops 1048576 | bytes 2100224 | tf_op jit(solution)/shard_map/convert_element_type | solution.py:456
  17.9 3.4 %all-to-all-start = ((bf16[4,128,256]{2,1,0:T(8,128)(2,1)}), bf16[4,128,256]{2,1,0:T(8,128)(2,1)S(1)}, u32[]{:S(2)}, u32[]{:S(2)}) async-start(bf16[4,128,256]{2,1,0:T(8,128)(2,1)} %bitcast.3), calls=%async_computation | async-start | bytes 524288 | tf_op jit(solution)/shard_map/all_to_all | solution.py:458
  21.4 0.0 copy-done.2
  21.4 0.0 copy-done.3
  21.4 0.0 copy-done.5
  21.4 0.7 copy.23.routes_ref
  22.2 0.0 copy-done.6
  22.2 0.7 copy.24.weights_ref
  22.9 0.0 copy-done.4
  22.9 0.6 reshape.24.post_ref
  23.5 7.1 %all-to-all-done = bf16[4,128,256]{2,1,0:T(8,128)(2,1)S(1)} async-done(((bf16[4,128,256]{2,1,0:T(8,128)(2,1)}), bf16[4,128,256]{2,1,0:T(8,128)(2,1)S(1)}, u32[]{:S(2)}, u32[]{:S(2)}) %all-to-all-start) | async-done | bytes 262176 | tf_op jit(solution)/shard_map/all_to_all | solution.py:458
  30.6 0.2 copy.22
  30.7 18.2 %all-gather.2.cloned.1.call-done = bf16[1024,2048]{1,0:T(8,128)(2,1)} async-done(((bf16[256,2048]{1,0:T(8,128)(2,1)}), bf16[1024,2048]{1,0:T(8,128)(2,1)}) %all-gather.2.cloned.1.call-update) | async-done | bytes 4194320 | tf_op jit(solution)/shard_map/all_gather | solution.py:461
  48.9 3.0 %multiply_reduce_fusion = (f32[128]{0:T(128)S(1)}, f32[128,2048]{1,0:T(8,128)S(1)}) fusion(bf16[128,1024]{0,1:T(8,128)(2,1)S(1)} %bitcast.8, bf16[1024,2048]{1,0:T(8,128)(2,1)} %all-gather.2.cloned.1.call-done), kind=kOutput, calls=%fused_computation.6 | convolution fusion | flops 537395072 | bytes 5505536 | tf_op jit(solution)/shard_map/dot_general | solution.py:459
  52.0 0.0 copy-done.1
  52.0 0.4 fusion
  52.3 0.0 copy-start
  52.4 1.0 fusion.2.normed_ref
  53.4 0.0 copy-done
  53.4 102.7 %shard_map.163 = bf16[128,2048]{1,0:T(8,128)(2,1)} custom-call(bf16[128,2048]{1,0:T(8,128)(2,1)} %fusion.2.normed_ref, bf16[128,2048]{1,0:T(8,128)(2,1)} %copy-done, s32[128,4]{1,0:T(8,128)} %copy.23.routes_ref, f32[128,4]{1,0:T(8,128)} %copy.24.weights_ref, bf16[1,2048]{1,0:T(2,128)(2,1)} %reshape.24.post_ref, bf16[1,2048,512]{2,1,0:T(8,128)(2,1)} %eg_ref.1, ...), custom_call_target="tpu_custom_call" | custom-call | tf_op jit(solution)/shard_map/pallas_call | solution.py:385
  156.1 1.9 %copy.26 = bf16[128,2048]{1,0:T(8,128)(2,1)} copy(bf16[128,2048]{1,0:T(8,128)(2,1)} %shard_map.163) | data formatting | bytes 1048576
  (6 shorter events, 0.0 us)
Async XLA Ops:
  6.5 14.8 %copy-start.2 = (bf16[2048]{0:T(1024)(128)(2,1)S(1)}, bf16[2048]{0:T(1024)(128)(2,1)}, u32[]{:S(2)}) copy-start(bf16[2048]{0:T(1024)(128)(2,1)} %param.22) | copy-start | bytes 12292
  6.5 14.9 %copy-start.3 = (bf16[2048]{0:T(1024)(128)(2,1)S(1)}, bf16[2048]{0:T(1024)(128)(2,1)}, u32[]{:S(2)}) copy-start(bf16[2048]{0:T(1024)(128)(2,1)} %param.24) | copy-start | bytes 12292
  6.5 14.9 %copy-start.5 = (s32[128,4]{0,1:T(4,128)S(1)}, s32[128,4]{0,1:T(4,128)}, u32[]{:S(2)}) copy-start(s32[128,4]{0,1:T(4,128)} %param.32) | copy-start | bytes 6148
  6.5 15.6 %copy-start.6 = (f32[128,4]{0,1:T(4,128)S(1)}, f32[128,4]{0,1:T(4,128)}, u32[]{:S(2)}) copy-start(f32[128,4]{0,1:T(4,128)} %param.33) | copy-start | bytes 6148
  6.5 16.3 %copy-start.4 = (bf16[2048]{0:T(1024)(128)(2,1)S(1)}, bf16[2048]{0:T(1024)(128)(2,1)}, u32[]{:S(2)}) copy-start(bf16[2048]{0:T(1024)(128)(2,1)} %param.31) | copy-start | bytes 12292
  6.5 42.4 %all-gather.2.cloned.1.call-start = ((), (), s32[]{:S(2)}) async-start(), calls=%async_computation.1 | async-start | bytes 5242880 | tf_op jit(solution)/shard_map/all_gather | solution.py:461
  8.7 6.2 %collective-permute-start = (bf16[2,512]{1,0:T(2,128)(2,1)S(1)}, bf16[2,512]{1,0:T(2,128)(2,1)S(1)}, u32[]{:S(2)}, u32[]{:S(2)}) collective-permute-start(bf16[2,512]{1,0:T(2,128)(2,1)S(1)} %pad_maximum_fusion), channel_id=1, source_target_pairs={{0,4},{4,8},{8,12},{12,16},{16,20},{20,24},{24,28},{1,5},{5,9},{9,... | collective-permute-start | bytes 6152 | tf_op jit(solution)/shard_map/ppermute | solution.py:422
  16.0 36.0 %copy-start.1 = (bf16[128,2048]{1,0:T(8,128)(2,1)S(1)}, bf16[128,2048]{1,0:T(8,128)(2,1)}, u32[]{:S(2)}) copy-start(bf16[128,2048]{1,0:T(8,128)(2,1)} %param.23) | copy-start | bytes 1572868
  17.9 12.6 %all-to-all-start = ((bf16[4,128,256]{2,1,0:T(8,128)(2,1)}), bf16[4,128,256]{2,1,0:T(8,128)(2,1)S(1)}, u32[]{:S(2)}, u32[]{:S(2)}) async-start(bf16[4,128,256]{2,1,0:T(8,128)(2,1)} %bitcast.3), calls=%async_computation | async-start | bytes 524288 | tf_op jit(solution)/shard_map/all_to_all | solution.py:458
  52.3 1.0 copy-start
Sparse Core Ops, SparseCore 0:
  8.9 39.9 all-gather.1

commit v2 on v1

--- a/solution.py
+++ b/solution.py
@@ -13,13 +13,17 @@
 HALVES = 2
 
 
-def moe_kernel(
+def layer_kernel(
     line,
-    normed_ref,
+    x_ref,
+    gate_b_ref,
+    gate_c_ref,
+    taps_ref,
     resid_ref,
+    gains_ref,
     routes_ref,
     weights_ref,
-    post_ref,
+    proj_ref,
     eg_ref,
     eu_ref,
     ed_ref,
@@ -27,6 +31,16 @@
     su_ref,
     sd_ref,
     out_ref,
+    edge_x,
+    edge_c,
+    mixed,
+    conv,
+    conv_near,
+    proj,
+    part_out,
+    part_in,
+    projected,
+    resid1,
     w_gate,
     w_up,
     w_down,
@@ -42,6 +56,14 @@
     shares,
     hidden,
     load_sem,
+    e_send,
+    e_recv,
+    p_send,
+    p_recv,
+    c_send,
+    c_recv,
+    f_send,
+    f_recv,
     wx_send,
     wx_recv,
     wn_send,
@@ -72,7 +94,7 @@
     near = (tp // 2) * 2 + 1 - tp % 2
     far = (tp + 2) % tp_size
     near_far = (near + 2) % tp_size
-    rows, width = normed_ref.shape
+    rows, width = resid_ref.shape
     step_rows = rows // PIECES
     hid = w_gate.shape[2]
     shared_hid = s_gate.shape[1]
@@ -93,12 +115,73 @@
                 (sg_ref, s_gate),
                 (su_ref, s_up),
                 (sd_ref, s_down),
+                (proj_ref, proj.at[0]),
             )
         )
     ]
-    for load in loads:
+    loads[-1].start()
+    for load in loads[:-1]:
         load.start()
+
+    all_rows, channels = x_ref.shape
+    reach = taps_ref.shape[0] - 1
+    pad = edge_x.shape[0]
+    mixed[pad:] = x_ref[...].astype(jnp.float32) * gate_c_ref[...].astype(jnp.float32)
+
+    def edge_copy(n):
+        source, landing = ((x_ref, edge_x), (gate_c_ref, edge_c))[n]
+        return pltpu.make_async_remote_copy(
+            src_ref=source.at[pl.ds(all_rows - pad, pad)],
+            dst_ref=landing,
+            send_sem=e_send.at[n],
+            recv_sem=e_recv.at[n],
+            device_id=((sp + 1) % sp_size, tp),
+            device_id_type=MESH,
+        )
+
+    proj_copy = pltpu.make_async_remote_copy(
+        src_ref=proj_ref,
+        dst_ref=proj.at[1],
+        send_sem=p_send.at[0],
+        recv_sem=p_recv.at[0],
+        device_id=(sp, near),
+        device_id_type=MESH,
+    )
+
+    def block_rows(owner):
+        return pl.ds(pl.multiple_of(owner * rows, rows), rows)
+
+    def conv_copy(n):
+        return pltpu.make_async_remote_copy(
+            src_ref=conv.at[block_rows((near, near_far)[n])],
+            dst_ref=conv_near.at[n],
+            send_sem=c_send.at[n],
+            recv_sem=c_recv.at[n],
+            device_id=(sp, near),
+            device_id_type=MESH,
+        )
+
+    part_cols = width // PIECES
+
+    def part_copy(j):
+        cols = pl.ds(pl.multiple_of(j * part_cols, part_cols), part_cols)
+        return pltpu.make_async_remote_copy(
+            src_ref=part_out.at[:, cols],
+            dst_ref=part_in.at[:, cols],
+            send_sem=f_send.at[j],
+            recv_sem=f_recv.at[j],
+            device_id=(sp, far),
+            device_id_type=MESH,
+        )
+
     pl.semaphore_wait(barrier, sp_size - 1 + tp_size - 1)
+
+    @pl.when(sp < sp_size - 1)
+    def _():
+        edge_copy(0).start()
+        edge_copy(1).start()
+
+    proj_copy.start()
 
     pieces = []
     for ref, held in ((eg_ref, w_gate), (eu_ref, w_up), (ed_ref, w_down)):
@@ -169,15 +252,74 @@
             device_id_type=MESH,
         )
 
+    for n in range(count):
+        x_hop(n).start()
+
     lanes = lax.broadcasted_iota(jnp.int32, (rows, shares.shape[2]), 1)
     table = jnp.zeros((rows, shares.shape[2]), jnp.float32)
     for k in range(routes_ref.shape[1]):
         table += jnp.where(lanes == routes_ref[:, k : k + 1], weights_ref[:, k : k + 1], 0.0)
     shares[z] = table
-    blocks[z] = normed_ref[...]
+
+    @pl.when(sp > 0)
+    def _():
+        edge_copy(0).wait_recv()
+        edge_copy(1).wait_recv()
+        mixed[:pad] = edge_x[...].astype(jnp.float32) * edge_c[...].astype(jnp.float32)
+
+    @pl.when(sp == 0)
+    def _():
+        mixed[:pad] = jnp.zeros((pad, channels), jnp.float32)
+
+    convolved = jnp.zeros((all_rows, channels), jnp.float32)
+    for k in range(reach + 1):
+        begin = pad - reach + k
+        convolved += taps_ref[k : k + 1].astype(jnp.float32) * mixed[begin : begin + all_rows]
+    conv[...] = (gate_b_ref[...].astype(jnp.float32) * convolved).astype(jnp.bfloat16)
+    conv_copy(1).start()
+    conv_copy(0).start()
+    for k in range(1, line):
+        share_copy(k, z).start()
+    loads[-1].wait()
+    proj_copy.wait_recv()
+
+    def project(n, owner, cols):
+        return jnp.dot(
+            conv[block_rows(owner)], proj[0, :, cols], preferred_element_type=jnp.float32
+        ) + jnp.dot(conv_near[n], proj[1, :, cols], preferred_element_type=jnp.float32)
+
+    conv_copy(1).wait_recv()
+
+    @pl.loop(0, PIECES)
+    def _(j):
+        cols = pl.ds(pl.multiple_of(j * part_cols, part_cols), part_cols)
+        part_out[:, cols] = project(1, far, cols).astype(jnp.bfloat16)
+        part_copy(j).start()
+
+    conv_copy(0).wait_recv()
+
+    @pl.loop(0, PIECES)
+    def _(j):
+        cols = pl.ds(pl.multiple_of(j * part_cols, part_cols), part_cols)
+        projected[:, cols] = project(0, tp, cols)
+
     sums[...] = jnp.zeros_like(sums)
-    for c in range(PIECES):
-
+
+    def spread(n):
+        x_hop(n).wait_recv()
+        far_hop(n, tp).start()
+        near_hop(n, tp).start()
+
+    for n in range(count // 2):
+        spread(n)
+
+    @pl.loop(0, PIECES)
+    def _(j):
+        cols = pl.ds(pl.multiple_of(j * part_cols, part_cols), part_cols)
+        part_copy(j).wait_recv()
+        projected[:, cols] += part_in[:, cols].astype(jnp.float32)
+
+    def send_block(c):
         @pl.when(z < last)
         def _():
             go_up(z, c).start()
@@ -186,10 +328,21 @@
         def _():
             go_down(z, c).start()
 
-    for n in range(count):
-        x_hop(n).start()
-    for k in range(1, line):
-        share_copy(k, z).start()
+    for c in range(PIECES):
+        part = pl.ds(c * step_rows, step_rows)
+        block = projected[part]
+        scale = lax.rsqrt(jnp.mean(block * block, axis=1, keepdims=True) + epsilon)
+        mid = (
+            resid_ref[part].astype(jnp.float32)
+            + block * scale * gains_ref[0:1].astype(jnp.float32)
+        ).astype(jnp.bfloat16)
+        resid1[part] = mid
+        wide = mid.astype(jnp.float32)
+        normal = lax.rsqrt(jnp.mean(wide * wide, axis=1, keepdims=True) + epsilon)
+        blocks[z, part] = (wide * normal * gains_ref[1:2].astype(jnp.float32)).astype(jnp.bfloat16)
+        if c > 0:
+            send_block(c - 1)
+    send_block(PIECES - 1)
 
     def apply(b, i):
         expert = z * 2 + x + i * (1 - 2 * x)
@@ -269,7 +422,7 @@
     for load in loads[:3]:
         load.wait()
     apply(z, 0)
-    for load in loads[3:]:
+    for load in loads[3:-1]:
         load.wait()
     s_g = jnp.dot(blocks[z], s_gate[...], preferred_element_type=jnp.float32)
     s_u = jnp.dot(blocks[z], s_up[...], preferred_element_type=jnp.float32)
@@ -283,34 +436,37 @@
             hidden[:, :shared_hid], s_down[:, cols], preferred_element_type=jnp.float32
         )
 
-    for n in range(count):
-        x_hop(n).wait_recv()
-        far_hop(n, tp).start()
-        near_hop(n, tp).start()
+    for n in range(count // 2, count):
+        spread(n)
     receive(1)
     for k in range(1, line):
         share_copy(k, (z + k) % line).wait_recv()
     apply_pair(1, 0)
-    for n in range(count):
+
+    def relay(n):
         far_hop(n, far).wait_recv()
         relay_hop(n, far).start()
-    receive(2)
+
+    for n in range(2 * count // 3):
+        relay(n)
+    for t in range(2, last):
+        receive(t)
+        apply_pair(t, 0)
+    for n in range(2 * count // 3, count):
+        relay(n)
     for n in range(count):
         near_hop(n, near).wait_recv()
         relay_hop(n, near_far).wait_recv()
-    apply_pair(1, 1)
-    give_back(1)
-
-    @pl.loop(2, line)
+
+    @pl.loop(1, last)
     def _(t):
-        @pl.when(t > 2)
-        def _():
-            receive(t)
-
-        apply_pair(t, 0)
         apply_pair(t, 1)
         give_back(t)
 
+    receive(last)
+    apply_pair(last, 0)
+    apply_pair(last, 1)
+    give_back(last)
     apply(z, 1)
 
     @pl.loop(line, 2 * line - 2)
@@ -334,10 +490,20 @@
         branch = sums[z, part] + shared[part]
         factor = lax.rsqrt(jnp.mean(branch * branch, axis=1, keepdims=True) + epsilon)
         out_ref[part] = (
-            resid_ref[part].astype(jnp.float32)
-            + branch * factor * post_ref[...].astype(jnp.float32)
+            resid1[part].astype(jnp.float32)
+            + branch * factor * gains_ref[2:3].astype(jnp.float32)
         ).astype(jnp.bfloat16)
 
+    @pl.when(sp < sp_size - 1)
+    def _():
+        edge_copy(0).wait_send()
+        edge_copy(1).wait_send()
+
+    proj_copy.wait_send()
+    conv_copy(0).wait_send()
+    conv_copy(1).wait_send()
+    for j in range(PIECES):
+        part_copy(j).wait_send()
     for n in range(count):
         x_hop(n).wait_send()
         near_hop(n, tp).wait_send()
@@ -367,27 +533,39 @@
                 back_down(b, c).wait_send()
 
 
-def routed_and_shared(
-    normed, resid1, routes, route_weights, post_gain, expert_gate, expert_up, expert_down,
-    shared_gate, shared_up, shared_down,
+def fused_layer(
+    x_in, gate_b, gate_c, conv_taps, out_proj, mix_gain, resid, pre_gain, expert_gate, expert_up,
+    expert_down, shared_gate, shared_up, shared_down, post_gain, routes, route_weights,
 ):
     experts = lax.axis_size("sp")
     line = experts // 2
-    rows, width = normed.shape
+    all_rows, channels = x_in.shape
+    rows, width = resid.shape
     hid = expert_gate.shape[2]
     shared_hid = shared_gate.shape[1]
     dma = pltpu.SemaphoreType.DMA
     count = 3 * HALVES
     bf, f32 = jnp.bfloat16, jnp.float32
     vmem = pl.BlockSpec(memory_space=pltpu.VMEM)
-    anywhere = pl.BlockSpec(memory_space=pltpu.HBM)
+    hbm = pl.BlockSpec(memory_space=pltpu.HBM)
     lanes = 128 * (-(-experts // 128))
+    pad = 16 * (-(-(conv_taps.shape[0] - 1) // 16))
     return pl.pallas_call(
-        functools.partial(moe_kernel, line),
+        functools.partial(layer_kernel, line),
         out_shape=jax.ShapeDtypeStruct((rows, width), bf),
-        in_specs=[vmem] * 5 + [anywhere] * 6,
+        in_specs=[vmem] * 8 + [hbm] * 7,
         out_specs=vmem,
         scratch_shapes=[
+            pltpu.VMEM((pad, channels), bf),
+            pltpu.VMEM((pad, channels), bf),
+            pltpu.VMEM((pad + all_rows, channels), f32),
+            pltpu.VMEM((all_rows, channels), bf),
+            pltpu.VMEM((2, rows, channels), bf),
+            pltpu.VMEM((2, channels, width), bf),
+            pltpu.VMEM((rows, width), bf),
+            pltpu.VMEM((rows, width), bf),
+            pltpu.VMEM((rows, width), f32),
+            pltpu.VMEM((rows, width), bf),
             pltpu.VMEM((2, width, hid), bf),
             pltpu.VMEM((2, width, hid), bf),
             pltpu.VMEM((2, hid, width), bf),
@@ -402,7 +580,15 @@
             pltpu.VMEM((line, rows, width), bf),
             pltpu.VMEM((line, rows, lanes), f32),
             pltpu.VMEM((rows, max(hid, shared_hid)), bf),
-            dma((6,)),
+            dma((7,)),
+            dma((2,)),
+            dma((2,)),
+            dma((1,)),
+            dma((1,)),
+            dma((2,)),
+            dma((2,)),
+            dma((PIECES,)),
+            dma((PIECES,)),
         ]
         + [dma((count,))] * 8
         + [dma((line,))] * 2
@@ -411,8 +597,9 @@
             collective_id=0, has_side_effects=True, vmem_limit_bytes=60 * 1024 * 1024
         ),
     )(
-        normed, resid1, routes, route_weights, post_gain.reshape(1, width),
-        expert_gate, expert_up, expert_down, shared_gate, shared_up, shared_down,
+        x_in, gate_b, gate_c, conv_taps, resid, jnp.stack([mix_gain, pre_gain, post_gain]),
+        routes, route_weights, out_proj, expert_gate, expert_up, expert_down,
+        shared_gate, shared_up, shared_down,
     )
 
 
@@ -441,6 +628,14 @@
     routes,
     route_weights,
 ):
+    group = lax.axis_size("sp")
+    wide_slots = 3 * resid.shape[0] * routes.shape[1] // group
+    if wide_slots > resid.shape[0] and group % 2 == 0 and lax.axis_size("tp") == 2 * 2:
+        return fused_layer(
+            x_in, gate_b, gate_c, conv_taps, out_proj, mix_gain, resid, pre_gain, expert_gate,
+            expert_up, expert_down, shared_gate, shared_up, shared_down, post_gain, routes,
+            route_weights,
+        )
     row_count = x_in.shape[0]
     channels = x_in.shape[1]
     reach = conv_taps.shape[0] - 1
@@ -475,11 +670,6 @@
     local_rows = resid.shape[0]
     top_count = routes.shape[1]
     capacity = 3 * local_rows * top_count // (2 * experts)
-    if 2 * capacity > local_rows and experts % 2 == 0 and lax.axis_size("tp") == 2 * 2:
-        return routed_and_shared(
-            normed, resid1, routes, route_weights, post_gain, expert_gate, expert_up, expert_down,
-            shared_gate, shared_up, shared_down,
-        )
     flat_ids = routes.reshape(-1)
     onehot = (flat_ids[:, None] == jnp.arange(experts, dtype=jnp.int32)[None, :]).astype(jnp.int32)
     before = jnp.cumsum(onehot, axis=0) - onehot

time: 165 us -> 121 us (0.73)
  waiting for transfers between devices: 26.5 us -> 0 us
  between operations: 13.5 us -> 0.01 us
  Pallas kernels: 103 us -> 113 us
  starting transfers between devices: 8.34 us -> 0 us
  other arithmetic: 4.46 us -> 0.63 us
  matrix products: 3 us -> 0 us
    all_gather x1 -> x0, waiting for transfers between devices: 18.2 us -> none  [body(): lax.all_gather(out_proj, 'tp', axis=0, tiled=True)]
    pallas_call x1, Pallas kernels: 103 us -> 113 us  [fused_layer(): pl.pallas_call(functools.partial(layer_kernel, line), out_shape=jax.Shape...]
    all_to_all x1 -> x0, waiting for transfers between devices: 7.09 us -> none  [body(): lax.all_to_all(conv_out, 'tp', split_axis=0, concat_axis=1, tiled=True)]
    ppermute x1 -> x0, starting transfers between devices: 4.87 us -> none  [passed_along(): return lax.ppermute(shard, axis, pairs)]
    all_to_all x1 -> x0, starting transfers between devices: 3.44 us -> none  [body(): lax.all_to_all(conv_out, 'tp', split_axis=0, concat_axis=1, tiled=True)]
    dot_general x1 -> x0, matrix products: 3 us -> none  [body(): jnp.dot(full_rows, lax.all_gather(out_proj, 'tp', axis=0, tiled=True), pr...]
    convert_element_type x4 -> x0, other arithmetic: 2.9 us -> none  [the longest x1 1.91 us: body(): conv_out = (gate_b.astype(jnp.float32) * convolved).astype(jnp.bfloat16)]
    slice x4 -> x0, local copies, waits for them, and re-layouts: 2.19 us -> none  [the longest x1 0.8 us: body(): taps[index][None, :] * mixed_in[index:index + row_count]]
  transfers between devices with their start and end apart: 3 -> 0, of which waited for: 3 -> 0; matrix products, arithmetic and copies ran while one was open for 5% -> 0% of each run, Pallas kernels for 0% -> 0%
where the time goes in v2:
time: 121 us
  Pallas kernels  113 us (93%)
  local copies, waits for them, and re-layouts  6.78 us (6%)
    pallas_call x1, Pallas kernels, fused_layer(): pl.pallas_call(functools.partial(layer_kernel, line), out_shape=jax.Shape...  113 us
    unnamed x3, local copies, waits for them, and re-layouts  4.7 us

profile of v2, /device:TPU:0, one launch (start us, length us, event | category | flops | bytes accessed | tf_op | source)
XLA Modules:
  0.0 120.9 jit_solution(10644367691918740311)
XLA Ops:
  0.0 0.7 stack.12
  0.7 0.7 stack.13
  1.4 0.7 stack.14
  2.1 0.6 pad_maximum_fusion.gains_ref
  2.7 1.4 %copy.18.routes_ref = s32[128,4]{1,0:T(8,128)} copy(s32[128,4]{0,1:T(4,128)} %param.32) | data formatting | bytes 4096 | tf_op args[15]
  4.1 1.4 %copy.19.weights_ref = f32[128,4]{1,0:T(8,128)} copy(f32[128,4]{0,1:T(4,128)} %param.33) | data formatting | bytes 4096 | tf_op args[16]
  5.5 113.4 %shard_map.163 = bf16[128,2048]{1,0:T(8,128)(2,1)} custom-call(bf16[512,256]{1,0:T(8,128)(2,1)} %x_ref.1, bf16[512,256]{1,0:T(8,128)(2,1)} %gate_b_ref.1, bf16[512,256]{1,0:T(8,128)(2,1)} %gate_c_ref.1, bf16[3,256]{1,0:T(4,128)(2,1)} %taps_ref.1, bf16[128,2048]{1,0:T(8,128)(2,1)} %resid_ref.1, bf16[3,2048]{1,0:T(4,128)(2,1)} %pad_maximum_fusion.gains_ref, ...), custom_call_target="tpu_custom_call" | custom-call | tf_op jit(solution)/shard_map/pallas_call | solution.py:553
  119.0 1.9 %copy.21 = bf16[128,2048]{1,0:T(8,128)(2,1)} copy(bf16[128,2048]{1,0:T(8,128)(2,1)} %shard_map.163) | data formatting | bytes 1048576

commit v3 on v2

--- a/solution.py
+++ b/solution.py
@@ -11,6 +11,7 @@
 epsilon = 1e-06
 PIECES = 4
 HALVES = 2
+DIRECT = 2
 
 
 def layer_kernel(
@@ -214,6 +215,9 @@
     def far_hop(n, owner):
         return hop(n, owner, (sp, far), wf_send, wf_recv)
 
+    def direct_hop(n):
+        return hop(n, far, (mate, tp), wf_send, wf_recv, True)
+
     def relay_hop(n, owner):
         return hop(n, owner, (sp, near), wr_send, wr_recv)
 
@@ -254,6 +258,8 @@
 
     for n in range(count):
         x_hop(n).start()
+    for n in range(count - DIRECT, count):
+        direct_hop(n).start()
 
     lanes = lax.broadcasted_iota(jnp.int32, (rows, shares.shape[2]), 1)
     table = jnp.zeros((rows, shares.shape[2]), jnp.float32)
@@ -307,7 +313,8 @@
 
     def spread(n):
         x_hop(n).wait_recv()
-        far_hop(n, tp).start()
+        if n < count - DIRECT:
+            far_hop(n, tp).start()
         near_hop(n, tp).start()
 
     for n in range(count // 2):
@@ -392,14 +399,18 @@
                 apply(b, i)
 
     def give_back(t):
-        b_up = t - z
-        b_down = 2 * last - z - t
+        p_up = t - z
+        p_down = t - (last - z)
+        b_up = (p_up + last) % last + 1
+        b_down = last - ((p_down + last) % last + 1)
+        send_up = (p_up >= 1) & (p_up <= last) & (b_up > z)
+        send_down = (p_down >= 1) & (p_down <= last) & (b_down < z)
 
         @pl.loop(0, PIECES)
         def _(c):
             part = pl.ds(pl.multiple_of(c * step_rows, step_rows), step_rows)
 
-            @pl.when((b_up > z) & (b_up <= last))
+            @pl.when(send_up)
             def _():
                 @pl.when(z > 0)
                 def _():
@@ -409,7 +420,7 @@
                 outgoing[b_up, part] = sums[b_up, part].astype(jnp.bfloat16)
                 back_up(b_up, c).start()
 
-            @pl.when((b_down < z) & (b_down >= 0))
+            @pl.when(send_down)
             def _():
                 @pl.when(z < last)
                 def _():
@@ -458,18 +469,19 @@
         near_hop(n, near).wait_recv()
         relay_hop(n, near_far).wait_recv()
 
-    @pl.loop(1, last)
+    @pl.loop(2, last)
     def _(t):
         apply_pair(t, 1)
-        give_back(t)
-
+
+    give_back(1)
+    apply_pair(1, 1)
     receive(last)
     apply_pair(last, 0)
     apply_pair(last, 1)
-    give_back(last)
+    give_back(2)
     apply(z, 1)
 
-    @pl.loop(line, 2 * line - 2)
+    @pl.loop(3, 2 * last - 1)
     def _(t):
         give_back(t)
 

time: 121 us -> 109 us (0.901); the launches traced: 121 us -> 107 us
  Pallas kernels: 113 us -> 100 us
    pallas_call x1, Pallas kernels: 113 us -> 100 us  [fused_layer(): pl.pallas_call(functools.partial(layer_kernel, line), out_shape=jax.Shape...]
where the time goes in v3:
time: 109 us; the launch traced here: 107 us
  Pallas kernels  100 us (92%)
  local copies, waits for them, and re-layouts  6.78 us (6%)
    pallas_call x1, Pallas kernels, fused_layer(): pl.pallas_call(functools.partial(layer_kernel, line), out_shape=jax.Shape...  100 us
    unnamed x3, local copies, waits for them, and re-layouts  4.7 us

profile of v3, /device:TPU:0, one launch (start us, length us, event | category | flops | bytes accessed | tf_op | source)
XLA Modules:
  0.0 107.4 jit_solution(3705305805073913260)
XLA Ops:
  0.0 0.7 stack.12
  0.7 0.7 stack.13
  1.4 0.7 stack.14
  2.1 0.6 pad_maximum_fusion.gains_ref
  2.7 1.4 %copy.18.routes_ref = s32[128,4]{1,0:T(8,128)} copy(s32[128,4]{0,1:T(4,128)} %param.32) | data formatting | bytes 4096 | tf_op args[15]
  4.1 1.4 %copy.19.weights_ref = f32[128,4]{1,0:T(8,128)} copy(f32[128,4]{0,1:T(4,128)} %param.33) | data formatting | bytes 4096 | tf_op args[16]
  5.5 100.0 %shard_map.163 = bf16[128,2048]{1,0:T(8,128)(2,1)} custom-call(bf16[512,256]{1,0:T(8,128)(2,1)} %x_ref.1, bf16[512,256]{1,0:T(8,128)(2,1)} %gate_b_ref.1, bf16[512,256]{1,0:T(8,128)(2,1)} %gate_c_ref.1, bf16[3,256]{1,0:T(4,128)(2,1)} %taps_ref.1, bf16[128,2048]{1,0:T(8,128)(2,1)} %resid_ref.1, bf16[3,2048]{1,0:T(4,128)(2,1)} %pad_maximum_fusion.gains_ref, ...), custom_call_target="tpu_custom_call" | custom-call | tf_op jit(solution)/shard_map/pallas_call | solution.py:565
  105.6 1.9 %copy.21 = bf16[128,2048]{1,0:T(8,128)(2,1)} copy(bf16[128,2048]{1,0:T(8,128)(2,1)} %shard_map.163) | data formatting | bytes 1048576
